TPU v7x, 32 devices: a whole 2x2x4 slice. The times are simulated.
32 devices in a mesh: rep: 2 (over x), fs: 8 (over z, y), tp: 2 (over core).
Axes of the slice: x: 2, y: 2, z: 4, core: 2. Of those that a mesh axis runs over, the one named last changes fastest.
Arguments:
- mixed_input: bfloat16 [8192, 1024], P(('rep', 'fs', 'tp')), may hold values from -6 to 6
- project_weight: bfloat16 [1024, 1024], P(('fs', 'tp')), may hold values from -0.1875 to 0.1875
- norm_gain: float32 [1024], replicated, may hold values from 0.1 to 1.9
- up_weight: bfloat16 [1024, 4096], P('fs', 'tp'), may hold values from -0.1875 to 0.1875
- down_weight: bfloat16 [4096, 1024], P('tp', 'fs'), may hold values from -0.09375 to 0.09375
Outputs:
- mlp_output: bfloat16 [8192, 1024], P(('rep', 'fs', 'tp'))
All inputs are finite; a program needn't handle non-finite values.
Results may differ from a plain program's by a relative error of at most 0.015.
Values may be sent and summed in bfloat16 or wider, within the bound.
A program may use at most 64 MiB of HBM per device.

v0:
```python
import jax
import jax.numpy as jnp
from jax import lax
from jax.sharding import PartitionSpec as P

epsilon = 1e-06


def gathered_then(section, axis, dim, apply):
    everything = lax.all_gather(section, axis, axis=dim, tiled=True)
    return apply(everything, jnp.int32(0))


def own_rows(contribution, width, axis):
    whole = contribution(jnp.int32(0), width * lax.axis_size(axis)).astype(jnp.bfloat16)
    return lax.psum_scatter(whole, axis, scatter_dimension=0, tiled=True).astype(jnp.float32)


def local(mixed_input, project_weight, norm_gain, up_weight, down_weight):
    whole_project = lax.all_gather(project_weight, ("fs", "tp"), axis=0, tiled=True)
    projected = jnp.dot(mixed_input, whole_project, preferred_element_type=jnp.float32).astype(
        jnp.bfloat16
    )
    values = projected.astype(jnp.float32)
    scale = lax.rsqrt(jnp.mean(values * values, axis=-1, keepdims=True) + epsilon)
    normed = (values * scale * norm_gain.astype(jnp.float32)).astype(jnp.bfloat16)
    up_full = lax.all_gather(up_weight, "fs", axis=0, tiled=True)
    down_full = lax.all_gather(down_weight, "fs", axis=1, tiled=True)

    def lifted(token_piece, first_row):
        preact = jnp.dot(token_piece, up_full, preferred_element_type=jnp.float32)
        return jnp.square(jax.nn.relu(preact)).astype(jnp.bfloat16)

    hidden = gathered_then(normed, "tp", 0, lifted)

    def partial_term(first_row, row_count):
        row_block = lax.dynamic_slice_in_dim(hidden, first_row, row_count, 0)
        return jnp.dot(row_block, down_full, preferred_element_type=jnp.float32)

    summed = own_rows(partial_term, mixed_input.shape[0], "tp")
    return summed.astype(jnp.bfloat16)


def solution(mesh):
    placed = (
        P(("rep", "fs", "tp"), None),
        P(("fs", "tp"), None),
        P(),
        P("fs", "tp"),
        P("tp", "fs"),
    )
    return jax.shard_map(
        local, mesh=mesh, in_specs=placed, out_specs=P(("rep", "fs", "tp"), None), check_vma=False
    )
```

profile of v0, /device:TPU:0, one launch (start us, length us, event | category | flops | bytes accessed | tf_op | source)
XLA Modules:
  0.0 239.4 jit_solution(3866611374542259978)
XLA Ops:
  6.5 0.0 copy-start
  6.5 0.0 all-gather.5.cloned.1.call-start
  6.5 0.7 all-gather.5.cloned.1.call-update
  7.3 0.0 all-gather.7.cloned.1.call-start
  7.3 46.4 %all-gather.5.cloned.1.call-done = bf16[1024,1024]{1,0:T(8,128)(2,1)} async-done(((bf16[64,1024]{1,0:T(8,128)(2,1)}), bf16[1024,1024]{1,0:T(8,128)(2,1)}) %all-gather.5.cloned.1.call-update) | async-done | bytes 2097168 | tf_op jit(solution)/shard_map/all_gather | solution.py:20
  53.7 0.0 copy-done
  53.7 2.4 fusion
  56.1 1.7 fusion.2
  57.8 0.0 all-gather.7.cloned.1.call-update
  57.8 0.0 all-gather.9.cloned.1.call-start
  57.9 0.7 all-gather.9.cloned.1.call-update
  58.5 0.0 all-gather.11.cloned.1.call-start
  58.6 0.5 all-gather.11.cloned.1.call-update
  59.1 0.0 reduce-scatter.2.cloned.1.call-start
  59.2 6.5 %all-gather.7.cloned.1.call-done = bf16[512,1024]{1,0:T(8,128)(2,1)} async-done(((bf16[256,1024]{1,0:T(8,128)(2,1)}), bf16[512,1024]{1,0:T(8,128)(2,1)}) %all-gather.7.cloned.1.call-update) | async-done | bytes 1048592 | tf_op jit(solution)/shard_map/all_gather | solution.py:10
  65.7 76.1 %all-gather.9.cloned.1.call-done = bf16[1024,2048]{1,0:T(8,128)(2,1)} async-done(((bf16[128,2048]{1,0:T(8,128)(2,1)}), bf16[1024,2048]{1,0:T(8,128)(2,1)}) %all-gather.9.cloned.1.call-update) | async-done | bytes 4194320 | tf_op jit(solution)/shard_map/all_gather | solution.py:27
  141.8 75.1 %all-gather.11.cloned.1.call-done = bf16[2048,1024]{1,0:T(8,128)(2,1)} async-done(((bf16[2048,128]{1,0:T(8,128)(2,1)}), bf16[2048,1024]{1,0:T(8,128)(2,1)}) %all-gather.11.cloned.1.call-update) | async-done | bytes 4194320 | tf_op jit(solution)/shard_map/all_gather | solution.py:28
  216.9 9.2 %convolution_convert_fusion = bf16[512,1024]{1,0:T(8,128)(2,1)} fusion(bf16[2048,1024]{1,0:T(8,128)(2,1)} %all-gather.11.cloned.1.call-done, bf16[512,1024]{1,0:T(8,128)(2,1)} %all-gather.7.cloned.1.call-done, bf16[1024,2048]{1,0:T(8,128)(2,1)} %all-gather.9.cloned.1.call-done), kind=kOutput, calls=%fused_computation.1 | convolution fusion | flops 4298637312 | bytes 10485760 | tf_op jit(solution)/shard_map/dot_general | solution.py:38
  226.2 0.0 reduce-scatter.2.cloned.1.call-update
  226.2 6.7 %reduce-scatter.2.cloned.1.call-done = bf16[256,1024]{1,0:T(8,128)(2,1)} async-done(((bf16[512,1024]{1,0:T(8,128)(2,1)}), bf16[256,1024]{1,0:T(8,128)(2,1)}) %reduce-scatter.2.cloned.1.call-update) | async-done | bytes 524304 | tf_op jit(solution)/shard_map/reduce_scatter | solution.py:16
  (1 shorter events, 0.0 us)
Async XLA Ops:
  6.5 47.2 %copy-start = (bf16[256,1024]{1,0:T(8,128)(2,1)S(1)}, bf16[256,1024]{1,0:T(8,128)(2,1)}, u32[]{:S(2)}) copy-start(bf16[256,1024]{1,0:T(8,128)(2,1)} %param.5) | copy-start | bytes 1572868
  6.5 47.2 %all-gather.5.cloned.1.call-start = ((), (), s32[]{:S(2)}) async-start(), calls=%async_computation.1 | async-start | bytes 2228224 | tf_op jit(solution)/shard_map/all_gather | solution.py:20
  7.3 58.4 %all-gather.7.cloned.1.call-start = ((), (), s32[]{:S(2)}) async-start(), calls=%async_computation.2 | async-start | bytes 1572864 | tf_op jit(solution)/shard_map/all_gather | solution.py:10
  57.8 84.0 %all-gather.9.cloned.1.call-start = ((), (), s32[]{:S(2)}) async-start(), calls=%async_computation.3 | async-start | bytes 4718592 | tf_op jit(solution)/shard_map/all_gather | solution.py:27
  58.5 158.4 %all-gather.11.cloned.1.call-start = ((), (), s32[]{:S(2)}) async-start(), calls=%async_computation.4 | async-start | bytes 4718592 | tf_op jit(solution)/shard_map/all_gather | solution.py:28
  59.1 173.8 %reduce-scatter.2.cloned.1.call-start = ((), (), s32[]{:S(2)}) async-start(), calls=%async_computation.5 | async-start | bytes 1572864 | tf_op jit(solution)/shard_map/reduce_scatter | solution.py:16
Sparse Core Ops, SparseCore 0:
  9.5 44.1 all-gather.4
  57.9 7.7 all-gather.6
  67.8 73.9 all-gather.8
  143.7 73.1 all-gather.10
  226.3 6.5 reduce-scatter.1
where the time goes:
time: 240 us; the launch traced here: 239 us
  waiting for transfers between devices  213 us (89%)
  between operations  13.1 us (5%)
  matrix products  11.6 us (5%)
    all_gather x1, waiting for transfers between devices, local(): up_full = lax.all_gather(up_weight, 'fs', axis=0, tiled=True)  76.1 us
    all_gather x1, waiting for transfers between devices, local(): down_full = lax.all_gather(down_weight, 'fs', axis=1, tiled=True)  75.1 us
    all_gather x1, waiting for transfers between devices, local(): lax.all_gather(project_weight, ('fs', 'tp'), axis=0, tiled=True)  46.4 us
    dot_general x1, matrix products, partial_term(): return jnp.dot(row_block, down_full, preferred_element_type=jnp.float32)  9.23 us
    reduce_scatter x1, waiting for transfers between devices, own_rows(): lax.psum_scatter(whole, axis, scatter_dimension=0, tiled=True)  6.73 us
    all_gather x1, waiting for transfers between devices, gathered_then(): everything = lax.all_gather(section, axis, axis=dim, tiled=True)  6.54 us
  transfers between devices with their start and end apart: 5, of which 5 were waited for; matrix products, arithmetic and copies ran while one was open for 0% of the time, Pallas kernels for 0%

commit v1 on v0

--- a/solution.py
+++ b/solution.py
@@ -24,7 +24,9 @@
     values = projected.astype(jnp.float32)
     scale = lax.rsqrt(jnp.mean(values * values, axis=-1, keepdims=True) + epsilon)
     normed = (values * scale * norm_gain.astype(jnp.float32)).astype(jnp.bfloat16)
-    up_full = lax.all_gather(up_weight, "fs", axis=0, tiled=True)
+    up_full = jnp.concatenate(
+        lax.all_to_all(jnp.stack([up_weight] * lax.axis_size("fs")), "fs", 0, 0), axis=0
+    )
     down_full = lax.all_gather(down_weight, "fs", axis=1, tiled=True)
 
     def lifted(token_piece, first_row):

time: 240 us -> 234 us (0.975)
  waiting for transfers between devices: 213 us -> 200 us
  starting transfers between devices: 0.16 us -> 4.69 us
  local copies, waits for them, and re-layouts: 0.01 us -> 2.52 us
    all_to_all x0 -> x1, waiting for transfers between devices: none -> 140 us  [local(): lax.all_to_all(jnp.stack([up_weight] * lax.axis_size('fs')), 'fs', 0, 0)]
    all_gather x1 -> x0, waiting for transfers between devices: 76.1 us -> none  [local(): up_full = lax.all_gather(up_weight, 'fs', axis=0, tiled=True)]
    all_gather x1, waiting for transfers between devices: 75.1 us -> 4.32 us  [local(): down_full = lax.all_gather(down_weight, 'fs', axis=1, tiled=True)]
    all_gather x1, waiting for transfers between devices: 6.54 us -> 0.02 us  [gathered_then(): everything = lax.all_gather(section, axis, axis=dim, tiled=True)]
    all_to_all x0 -> x1, starting transfers between devices: none -> 4.57 us  [local(): lax.all_to_all(jnp.stack([up_weight] * lax.axis_size('fs')), 'fs', 0, 0)]
    another operation x0 -> x1, local copies, waits for them, and re-layouts: none -> 2.52 us  [local(): jnp.stack([up_weight] * lax.axis_size('fs'))]
  transfers between devices with their start and end apart: 5 -> 5, of which waited for: 5 -> 4; matrix products, arithmetic and copies ran while one was open for 0% -> 1% of each run, Pallas kernels for 0% -> 0%
where the time goes in v1:
time: 234 us
  waiting for transfers between devices  200 us (85%)
  between operations  13.2 us (6%)
  matrix products  11.7 us (5%)
  starting transfers between devices  4.69 us (2%)
  local copies, waits for them, and re-layouts  2.52 us (1%)
    all_to_all x1, waiting for transfers between devices, local(): lax.all_to_all(jnp.stack([up_weight] * lax.axis_size('fs')), 'fs', 0, 0)  140 us
    all_gather x1, waiting for transfers between devices, local(): lax.all_gather(project_weight, ('fs', 'tp'), axis=0, tiled=True)  46.4 us
    dot_general x1, matrix products, partial_term(): return jnp.dot(row_block, down_full, preferred_element_type=jnp.float32)  9.34 us
    reduce_scatter x1, waiting for transfers between devices, own_rows(): lax.psum_scatter(whole, axis, scatter_dimension=0, tiled=True)  8.44 us
  transfers between devices with their start and end apart: 5, of which 4 were waited for; matrix products, arithmetic and copies ran while one was open for 1% of the time, Pallas kernels for 0%

profile of v1, /device:TPU:0, one launch (start us, length us, event | category | flops | bytes accessed | tf_op | source)
XLA Modules:
  0.0 234.0 jit_solution(1823996413926738483)
XLA Ops:
  6.5 0.0 copy-start
  6.5 0.0 copy-start.1
  6.5 0.0 all-gather.4.cloned.1.call-start
  6.5 0.7 all-gather.4.cloned.1.call-update
  7.3 0.0 all-gather.6.cloned.1.call-start
  7.3 46.4 %all-gather.4.cloned.1.call-done = bf16[1024,1024]{1,0:T(8,128)(2,1)} async-done(((bf16[64,1024]{1,0:T(8,128)(2,1)}), bf16[1024,1024]{1,0:T(8,128)(2,1)}) %all-gather.4.cloned.1.call-update) | async-done | bytes 2097168 | tf_op jit(solution)/shard_map/all_gather | solution.py:20
  53.7 0.0 copy-done
  53.7 2.4 %fusion = (f32[256]{0:T(256)S(1)}, bf16[256,1024]{1,0:T(8,128)(2,1)S(1)}) fusion(bf16[256,1024]{1,0:T(8,128)(2,1)S(1)} %copy-done, bf16[1024,1024]{1,0:T(8,128)(2,1)} %all-gather.4.cloned.1.call-done), kind=kOutput, calls=%fused_computation.5 | convolution fusion | flops 537919232 | bytes 3146752 | tf_op jit(solution)/shard_map/dot_general | solution.py:21
  56.1 1.7 fusion.2
  57.8 0.0 all-gather.6.cloned.1.call-update
  57.8 0.0 copy-done.1
  57.8 2.5 %stack.2 = bf16[8,128,2048]{2,1,0:T(8,128)(2,1)} broadcast(bf16[128,2048]{1,0:T(8,128)(2,1)S(1)} %copy-done.1), dimensions={1,2} | broadcast | bytes 4718592 | tf_op jit(solution)/shard_map/stack | solution.py:28
  60.3 4.6 %all-to-all-start = ((bf16[8,128,2048]{2,1,0:T(8,128)(2,1)}), bf16[8,128,2048]{2,1,0:T(8,128)(2,1)}, u32[]{:S(2)}, u32[]{:S(2)}) async-start(bf16[8,128,2048]{2,1,0:T(8,128)(2,1)} %stack.2), calls=%async_computation | async-start | bytes 8388608 | tf_op jit(solution)/shard_map/all_to_all | solution.py:28
  64.9 0.0 all-gather.8.cloned.1.call-start
  65.0 0.7 all-gather.8.cloned.1.call-update
  65.7 0.0 reduce-scatter.2.cloned.1.call-start
  65.7 0.0 all-gather.6.cloned.1.call-done
  65.7 139.6 %all-to-all-done = bf16[8,128,2048]{2,1,0:T(8,128)(2,1)} async-done(((bf16[8,128,2048]{2,1,0:T(8,128)(2,1)}), bf16[8,128,2048]{2,1,0:T(8,128)(2,1)}, u32[]{:S(2)}, u32[]{:S(2)}) %all-to-all-start) | async-done | bytes 4194336 | tf_op jit(solution)/shard_map/all_to_all | solution.py:28
  205.3 4.3 %all-gather.8.cloned.1.call-done = bf16[2048,1024]{1,0:T(8,128)(2,1)} async-done(((bf16[2048,128]{1,0:T(8,128)(2,1)}), bf16[2048,1024]{1,0:T(8,128)(2,1)}) %all-gather.8.cloned.1.call-update) | async-done | bytes 4194320 | tf_op jit(solution)/shard_map/all_gather | solution.py:30
  209.6 9.3 %convolution_convert_fusion = bf16[512,1024]{1,0:T(8,128)(2,1)} fusion(bf16[2048,1024]{1,0:T(8,128)(2,1)} %all-gather.8.cloned.1.call-done, bf16[512,1024]{1,0:T(8,128)(2,1)} %all-gather.6.cloned.1.call-done, bf16[1024,2048]{1,0:T(8,128)(2,1)} %bitcast), kind=kOutput, calls=%fused_computation.1 | convolution fusion | flops 4298637312 | bytes 10485760 | tf_op jit(solution)/shard_map/dot_general | solution.py:40
  219.0 0.0 reduce-scatter.2.cloned.1.call-update
  219.0 8.4 %reduce-scatter.2.cloned.1.call-done = bf16[256,1024]{1,0:T(8,128)(2,1)} async-done(((bf16[512,1024]{1,0:T(8,128)(2,1)}), bf16[256,1024]{1,0:T(8,128)(2,1)}) %reduce-scatter.2.cloned.1.call-update) | async-done | bytes 524304 | tf_op jit(solution)/shard_map/reduce_scatter | solution.py:16
  (1 shorter events, 0.0 us)
Async XLA Ops:
  6.5 47.2 %copy-start = (bf16[256,1024]{1,0:T(8,128)(2,1)S(1)}, bf16[256,1024]{1,0:T(8,128)(2,1)}, u32[]{:S(2)}) copy-start(bf16[256,1024]{1,0:T(8,128)(2,1)} %param.5) | copy-start | bytes 1572868
  6.5 51.3 %copy-start.1 = (bf16[128,2048]{1,0:T(8,128)(2,1)S(1)}, bf16[128,2048]{1,0:T(8,128)(2,1)}, u32[]{:S(2)}) copy-start(bf16[128,2048]{1,0:T(8,128)(2,1)} %param.8) | copy-start | bytes 1572868
  6.5 47.2 %all-gather.4.cloned.1.call-start = ((), (), s32[]{:S(2)}) async-start(), calls=%async_computation.2 | async-start | bytes 2228224 | tf_op jit(solution)/shard_map/all_gather | solution.py:20
  7.3 58.5 %all-gather.6.cloned.1.call-start = ((), (), s32[]{:S(2)}) async-start(), calls=%async_computation.3 | async-start | bytes 1572864 | tf_op jit(solution)/shard_map/all_gather | solution.py:10
  60.3 145.0 %all-to-all-start = ((bf16[8,128,2048]{2,1,0:T(8,128)(2,1)}), bf16[8,128,2048]{2,1,0:T(8,128)(2,1)}, u32[]{:S(2)}, u32[]{:S(2)}) async-start(bf16[8,128,2048]{2,1,0:T(8,128)(2,1)} %stack.2), calls=%async_computation | async-start | bytes 8388608 | tf_op jit(solution)/shard_map/all_to_all | solution.py:28
  64.9 144.7 %all-gather.8.cloned.1.call-start = ((), (), s32[]{:S(2)}) async-start(), calls=%async_computation.4 | async-start | bytes 4718592 | tf_op jit(solution)/shard_map/all_gather | solution.py:30
  65.7 161.8 %reduce-scatter.2.cloned.1.call-start = ((), (), s32[]{:S(2)}) async-start(), calls=%async_computation.5 | async-start | bytes 1572864 | tf_op jit(solution)/shard_map/reduce_scatter | solution.py:16
Sparse Core Ops, SparseCore 0:
  9.5 44.1 all-gather.3
  57.9 7.7 all-gather.5
  67.8 141.8 all-gather.7
  219.1 8.2 reduce-scatter.1
